TPU v7x, 32 devices: a whole 2x2x4 slice. The times are simulated.
32 devices in a mesh: ep: 8 (over z, x), tp: 4 (over y, core).
Axes of the slice: x: 2, y: 2, z: 4, core: 2. Of those that a mesh axis runs over, the one named last changes fastest.
Arguments:
- tokens: bfloat16 [128, 2048], P('ep'), may hold values from -6 to 6
- lengths: int32 [128], P('ep'), may hold values from 1 to 1024, as said below
- key_cache: bfloat16 [128, 1024, 8, 128], P('ep', None, 'tp'), may hold values from -200 to 200
- value_cache: bfloat16 [128, 1024, 8, 128], P('ep', None, 'tp'), may hold values from -6 to 6
- attn_gain: float32 [2048], replicated, may hold values from 0.1 to 1.9
- w_query: bfloat16 [2048, 8, 128], P(None, 'tp'), may hold values from -0.1875 to 0.1875
- w_key: bfloat16 [2048, 8, 128], P(None, 'tp'), may hold values from -0.15625 to 0.15625
- w_value: bfloat16 [2048, 8, 128], P(None, 'tp'), may hold values from -0.125 to 0.125
- mix_lambda: float32 [8], P('tp'), may hold values from 0.3 to 0.8
- head_gain: float32 [128], replicated, may hold values from 0.1 to 1.9
- w_out: bfloat16 [8, 128, 2048], P('tp'), may hold values from -2.5 to 2.5
- ffn_gain: float32 [2048], replicated, may hold values from 0.1 to 1.9
- w_gate: bfloat16 [8, 2048, 2048], P('ep', None, 'tp'), may hold values from -1 to 1
- w_up: bfloat16 [8, 2048, 2048], P('ep', None, 'tp'), may hold values from -1 to 1
- w_down: bfloat16 [8, 2048, 2048], P('ep', 'tp'), may hold values from -0.046875 to 0.046875
- routes: int32 [128, 4], P('ep'), may hold values from 0 to 7, all different within a row; in each aligned block of 16 rows (0 to 15, 16 to 31, ...) at most 16 rows name the same one
- route_weights: float32 [128, 4], P('ep'), may hold values from 0.1 to 1
Outputs:
- mixed: bfloat16 [128, 2048], P('ep', 'tp')
Inputs may be any that keep to these rules, and one draw needn't show every extreme that they name: `routes`: in each aligned block of 16 rows no expert is named by more than 16 entries, and one is named by exactly 16 in some block; each row names 4 different experts. `lengths`: some sequence has all 1024 positions valid.
All inputs are finite; a program needn't handle non-finite values.
Results may differ from a plain program's by a relative error of at most 0.02.
The roundings to bfloat16 on the way count: a program that leaves them out, or rounds other values in their place, can miss the bound.
Values may be sent and summed in bfloat16 or wider, within the bound.
No kernel may reach another device: no remote copies, remote signals or barrier semaphores. Data moves between devices by JAX's collectives and lax.ppermute only.
A program may use at most 128 MiB of HBM per device.

v0:
```python
import jax
import jax.numpy as jnp
from jax import lax
from jax.sharding import PartitionSpec as P

epsilon = 1e-06
clamp_limit = 7.0
sigmoid_slope = 1.702
branch_scale = 0.2


def norm_rows(source, gain):
    wide = source.astype(jnp.float32)
    return wide * lax.rsqrt(jnp.mean(wide * wide, axis=-1, keepdims=True) + epsilon) * gain


def mixed_weights(scores, own_scores, mix_lambda):
    peak = jnp.maximum(jnp.max(scores, axis=-1), own_scores)
    weights = jnp.exp(scores - peak[..., None])
    own_weight = jnp.exp(own_scores - peak)
    denominator = jnp.sum(weights, axis=-1) + own_weight
    shares = weights / denominator[..., None]
    own_share = own_weight / denominator
    balance = mix_lambda[None, :]
    mix_weights = (shares[:, :, 0] - balance[..., None] * shares[:, :, 1]).astype(jnp.bfloat16)
    own_mixed = (own_share[:, :, 0] - balance * own_share[:, :, 1]).astype(jnp.bfloat16)
    return (mix_weights, own_mixed)


def per_device(
    tokens,
    lengths,
    key_cache,
    value_cache,
    attn_gain,
    w_query,
    w_key,
    w_value,
    mix_lambda,
    head_gain,
    w_out,
    ffn_gain,
    w_gate,
    w_up,
    w_down,
    routes,
    route_weights,
):
    seq_dev, model_width = tokens.shape
    group_heads = w_query.shape[1]
    head_width = w_query.shape[2]
    half_width = head_width // 2
    columns = group_heads * head_width
    cache_len = key_cache.shape[1]
    normed = norm_rows(tokens, attn_gain).astype(jnp.bfloat16)
    queries = (
        jnp.dot(normed, w_query.reshape(model_width, columns), preferred_element_type=jnp.float32)
        .astype(jnp.bfloat16)
        .reshape(seq_dev, group_heads, head_width)
    )
    key_new = (
        jnp.dot(normed, w_key.reshape(model_width, columns), preferred_element_type=jnp.float32)
        .astype(jnp.bfloat16)
        .reshape(seq_dev, group_heads, head_width)
    )
    value_new = (
        jnp.dot(normed, w_value.reshape(model_width, columns), preferred_element_type=jnp.float32)
        .astype(jnp.bfloat16)
        .reshape(seq_dev, group_heads, head_width)
    )
    halves = (lax.iota(jnp.int32, head_width) < half_width).astype(jnp.bfloat16)
    stacked_query = jnp.stack([queries * halves, queries * (1 - halves)], axis=2)
    score_scale = half_width ** (-0.5)
    own_scores = (
        jnp.einsum("shcd,shd->shc", stacked_query, key_new, preferred_element_type=jnp.float32)
        * score_scale
    )
    positions = lax.iota(jnp.int32, cache_len)
    live_mask = (positions[None, :] < lengths[:, None])[:, None, None, :]
    scores = (
        jnp.einsum("shcd,slhd->shcl", stacked_query, key_cache, preferred_element_type=jnp.float32)
        * score_scale
    )
    scores = jnp.where(live_mask, scores, -jnp.inf)
    mix_weights, own_mixed = mixed_weights(scores, own_scores, mix_lambda)
    heads_out = jnp.einsum(
        "shl,slhd->shd", mix_weights, value_cache, preferred_element_type=jnp.float32
    )
    heads_out = heads_out + own_mixed.astype(jnp.float32)[..., None] * value_new.astype(jnp.float32)
    normed_heads = (
        heads_out
        * lax.rsqrt(jnp.mean(heads_out * heads_out, axis=-1, keepdims=True) + epsilon)
        * head_gain
        * branch_scale
    ).astype(jnp.bfloat16)
    partial_value = jnp.dot(
        normed_heads.reshape(seq_dev, columns),
        w_out.reshape(columns, model_width),
        preferred_element_type=jnp.float32,
    )
    partial_value = lax.optimization_barrier(partial_value.astype(jnp.bfloat16)).astype(jnp.float32)
    attention = lax.psum(partial_value.astype(jnp.bfloat16), "tp").astype(jnp.float32)
    residual = (tokens.astype(jnp.float32) + attention).astype(jnp.bfloat16)
    normed_ffn = norm_rows(residual, ffn_gain).astype(jnp.bfloat16)
    experts = lax.axis_size("ep")
    top_count = routes.shape[1]
    capacity = 2 * seq_dev * top_count // experts
    entries = routes.reshape(-1)
    onehot = (entries[:, None] == lax.iota(jnp.int32, experts)[None, :]).astype(jnp.int32)
    entry_slot = jnp.sum((jnp.cumsum(onehot, axis=0) - onehot) * onehot, axis=-1)
    target = entries * capacity + entry_slot
    slot_ids = lax.iota(jnp.int32, experts * capacity)
    placing = (slot_ids[:, None] == target[None, :]).astype(jnp.bfloat16)
    repeated = jnp.repeat(normed_ffn, top_count, axis=0)
    outgoing = jnp.dot(placing, repeated, preferred_element_type=jnp.float32).astype(jnp.bfloat16)
    outgoing = outgoing.reshape(experts, capacity, model_width)
    block_cols = model_width // lax.axis_size("tp")
    own_block = lax.dynamic_slice_in_dim(outgoing, lax.axis_index("tp") * block_cols, block_cols, 2)
    arrived = lax.all_gather(
        lax.all_to_all(own_block, "ep", split_axis=0, concat_axis=0, tiled=True),
        "tp",
        axis=2,
        tiled=True,
    )
    sources, slot_count, _ = arrived.shape
    flat_rows = arrived.reshape(sources * slot_count, model_width)
    gate_value = jnp.minimum(
        jnp.dot(flat_rows, w_gate[0], preferred_element_type=jnp.float32), clamp_limit
    )
    up_value = jnp.clip(
        jnp.dot(flat_rows, w_up[0], preferred_element_type=jnp.float32), -clamp_limit, clamp_limit
    )
    activated = ((up_value + 1.0) * gate_value * jax.nn.sigmoid(sigmoid_slope * gate_value)).astype(
        jnp.bfloat16
    )
    pieces = jnp.dot(activated, w_down[0], preferred_element_type=jnp.float32)
    pieces = lax.optimization_barrier(pieces.astype(jnp.bfloat16)).astype(jnp.float32)
    summed = lax.psum_scatter(
        pieces.reshape(sources, slot_count, model_width).astype(jnp.bfloat16),
        "tp",
        scatter_dimension=2,
        tiled=True,
    )
    returned = lax.all_to_all(summed, "ep", split_axis=0, concat_axis=0, tiled=True)
    slice_width = returned.shape[2]
    returned = returned.reshape(experts * capacity, slice_width).astype(jnp.float32)
    chosen = (target.reshape(seq_dev, top_count)[..., None] == slot_ids[None, None, :]).astype(
        jnp.float32
    )
    combine = jnp.sum(route_weights[..., None] * chosen, axis=1)
    expert_sum = jnp.dot(combine, returned, precision=lax.Precision.HIGHEST)
    own_columns = lax.dynamic_slice_in_dim(
        residual, lax.axis_index("tp") * slice_width, slice_width, 1
    )
    return (own_columns.astype(jnp.float32) + expert_sum).astype(jnp.bfloat16)


def solution(mesh):
    placed = (
        P("ep", None),
        P("ep"),
        P("ep", None, "tp", None),
        P("ep", None, "tp", None),
        P(),
        P(None, "tp", None),
        P(None, "tp", None),
        P(None, "tp", None),
        P("tp"),
        P(),
        P("tp", None, None),
        P(),
        P("ep", None, "tp"),
        P("ep", None, "tp"),
        P("ep", "tp", None),
        P("ep", None),
        P("ep", None),
    )
    return jax.shard_map(
        per_device, mesh=mesh, in_specs=placed, out_specs=P("ep", "tp"), check_vma=False
    )
```

profile of v0, /device:TPU:0, one launch (start us, length us, event | category | flops | bytes accessed | tf_op | source)
XLA Modules:
  0.0 125.2 jit_solution(6556066839307545895)
XLA Ops:
  6.6 1.1 fusion.55
  7.7 1.6 %convolution_convert_fusion.4 = bf16[16,256]{1,0:T(8,128)(2,1)S(1)} fusion(bf16[256,8,2,128]{3,2,1,0:T(2,128)(2,1)} %bitcast.110, bf16[16,2048]{1,0:T(8,128)(2,1)} %param.17, f32[2048]{0:T(1024)} %param.21, f32[16]{0:T(128)S(1)} %add_rsqrt_fusion.2), kind=kOutput, calls=%fused_computation.26 | convolution fusion | flops 16912384 | bytes 1130560 | tf_op jit(solution)/shard_map/dot_general | solution.py:57
  9.3 1.6 %convolution_convert_fusion.3 = bf16[16,256]{1,0:T(8,128)(2,1)S(1)} fusion(bf16[256,8,2,128]{3,2,1,0:T(2,128)(2,1)} %bitcast.111, bf16[16,2048]{1,0:T(8,128)(2,1)} %param.17, f32[2048]{0:T(1024)} %param.21, f32[16]{0:T(128)S(1)} %add_rsqrt_fusion.2), kind=kOutput, calls=%fused_computation.25 | convolution fusion | flops 16912384 | bytes 1130560 | tf_op jit(solution)/shard_map/dot_general | solution.py:62
  11.0 0.1 fusion.90
  11.1 0.1 copy.68
  11.2 0.1 iota_compare_fusion.1
  11.3 0.0 copy-start.9
  11.3 0.0 copy-start.10
  11.3 5.8 %fusion.89 = (f32[16,2,2]{2,1,0:T(2,128)S(1)}, f32[16,2,2,1024]{3,2,1,0:T(2,128)S(1)}) fusion(bf16[16,2,2,128]{3,2,1,0:T(2,128)(2,1)S(1)} %pad_maximum_fusion, bf16[16,1024,2,128]{3,2,1,0:T(2,128)(2,1)} %param.19, pred[16,1024]{1,0:T(8,128)(4,1)S(1)} %iota_compare_fusion.1), kind=kOutput, calls=%fused_computation.105 | convolution fusion | flops 16973760 | bytes 8683776 | tf_op jit(solution)/shard_map/shcd,slhd->shcl/dot_general | solution.py:81
  17.2 0.0 copy-start.5
  17.2 0.1 copy.59
  17.3 0.1 copy.60
  17.4 0.3 fusion.51
  17.7 0.1 copy.61
  17.8 0.1 copy.62
  17.9 0.3 fusion.50
  18.2 0.2 fusion.88
  18.5 0.3 fusion.35
  18.8 0.1 bitcast_convert_fusion
  18.8 0.2 fusion.66
  19.1 4.8 %fusion = f32[16,2,1,128]{3,2,1,0:T(1,128)S(1)} fusion(bf16[16,1024,2,128]{3,2,1,0:T(2,128)(2,1)} %param.20, bf16[16,2,1024,1]{2,1,0,3:T(2,128)(2,1)S(1)} %fusion.66), kind=kOutput, calls=%fused_computation | convolution fusion | flops 8388608 | bytes 8470528 | tf_op jit(solution)/shard_map/shl,slhd->shd/dot_general | solution.py:86
  23.9 0.2 multiply_reduce_fusion
  24.1 0.9 fusion.4
  25.0 0.0 all-reduce.2.cloned.1.call-update
  25.0 0.0 reduce-scatter.2.cloned.1.call-start
  25.1 0.1 copy.65
  25.1 0.1 eq.20
  25.2 0.1 fusion.68
  25.3 0.1 reduce_window_sum.11
  25.4 0.2 select_reduce_fusion.1
  25.6 33.8 %all-reduce.2.cloned.1.call-done = bf16[16,2048]{1,0:T(8,128)(2,1)} async-done(((bf16[16,2048]{1,0:T(8,128)(2,1)}), bf16[16,2048]{1,0:T(8,128)(2,1)}) %all-reduce.2.cloned.1.call-update) | async-done | bytes 65552 | tf_op jit(solution)/shard_map/psum | solution.py:102
  59.4 1.0 fusion.52
  60.4 0.1 fusion.54
  60.5 0.1 broadcast_in_dim.16
  60.6 0.1 reshape.137
  60.7 0.3 convolution_convert_fusion.1
  61.0 12.7 %all_to_all.10 = bf16[8,16,512]{2,1,0:T(8,128)(2,1)S(1)} all-to-all(bf16[8,16,512]{2,1,0:T(8,128)(2,1)S(1)} %constant_dynamic-slice_fusion), channel_id=1, replica_groups=mesh['ep'=8,'tp'=4] {'ep'}, dimensions={0} | all-to-all | bytes 262144 | tf_op jit(solution)/shard_map/all_to_all | solution.py:120
  73.6 6.5 %all_gather.3 = bf16[8,16,2048]{2,1,0:T(8,128)(2,1)S(1)} all-gather(bf16[8,16,512]{2,1,0:T(8,128)(2,1)S(1)} %all_to_all.10), channel_id=1, replica_groups=mesh['ep'=8,'tp'=4] {'tp'}, dimensions={2}, use_global_device_ids=true | all-gather | bytes 655360 | tf_op jit(solution)/shard_map/all_gather | solution.py:119
  80.1 2.0 %fusion.13 = f32[128,512]{1,0:T(8,128)S(1)} fusion(bf16[128,2048]{1,0:T(8,128)(2,1)S(1)} %bitcast.105, bf16[1,2048,512]{2,1,0:T(8,128)(2,1)} %param.29), kind=kOutput, calls=%fused_computation.14 | convolution fusion | flops 268500992 | bytes 2883584 | tf_op jit(solution)/shard_map/dot_general | solution.py:128
  82.2 3.2 %convolution_convert_fusion = bf16[128,2048]{1,0:T(8,128)(2,1)} fusion(bf16[1,512,2048]{2,1,0:T(8,128)(2,1)S(1)} %copy-done, f32[128,512]{1,0:T(8,128)S(1)} %fusion.13, bf16[128,2048]{1,0:T(8,128)(2,1)S(1)} %bitcast.106, bf16[1,2048,512]{2,1,0:T(8,128)(2,1)} %param.30), kind=kOutput, calls=%fused_computation.4 | convolution fusion | flops 537722880 | bytes 5505024 | tf_op jit(solution)/shard_map/dot_general | solution.py:136
  85.4 0.0 reduce-scatter.2.cloned.1.call-update
  85.4 0.1 reduce_sum.60
  85.5 0.1 copy.66
  85.6 19.2 %reduce-scatter.2.cloned.1.call-done = bf16[8,16,512]{2,1,0:T(8,128)(2,1)} async-done(((bf16[8,16,2048]{2,1,0:T(8,128)(2,1)}), bf16[8,16,512]{2,1,0:T(8,128)(2,1)}) %reduce-scatter.2.cloned.1.call-update) | async-done | bytes 131088 | tf_op jit(solution)/shard_map/reduce_scatter | solution.py:138
  104.8 5.5 %all-to-all-start.1 = ((bf16[8,16,512]{2,1,0:T(8,128)(2,1)}), bf16[8,16,512]{2,1,0:T(8,128)(2,1)S(1)}, u32[]{:S(2)}, u32[]{:S(2)}) async-start(bf16[8,16,512]{2,1,0:T(8,128)(2,1)} %reduce-scatter.2.cloned.1.call-done), calls=%async_computation.2 | async-start | bytes 262144 | tf_op jit(solution)/shard_map/all_to_all | solution.py:144
  110.3 0.1 select_reduce_fusion
  110.4 7.2 %all-to-all-done.1 = bf16[8,16,512]{2,1,0:T(8,128)(2,1)S(1)} async-done(((bf16[8,16,512]{2,1,0:T(8,128)(2,1)}), bf16[8,16,512]{2,1,0:T(8,128)(2,1)S(1)}, u32[]{:S(2)}, u32[]{:S(2)}) %all-to-all-start.1) | async-done | bytes 131104 | tf_op jit(solution)/shard_map/all_to_all | solution.py:144
  117.6 0.8 fusion.33
  (34 shorter events, 0.2 us)
Async XLA Ops:
  6.5 75.6 %copy-start = (bf16[1,512,2048]{2,1,0:T(8,128)(2,1)S(1)}, bf16[1,512,2048]{2,1,0:T(8,128)(2,1)}, u32[]{:S(2)}) copy-start(bf16[1,512,2048]{2,1,0:T(8,128)(2,1)} %param.31) | copy-start | bytes 6291460
  6.5 4.7 %copy-start.8 = (s32[16]{0:T(128)S(1)}, s32[16]{0:T(128)}, u32[]{:S(2)}) copy-start(s32[16]{0:T(128)} %param.18) | copy-start | bytes 196
  6.5 52.9 %all-reduce.2.cloned.1.call-start = ((), (), s32[]{:S(2)}) async-start(), calls=%async_computation.3 | async-start | bytes 131072 | tf_op jit(solution)/shard_map/psum | solution.py:102
  11.3 7.2 %copy-start.2 = (bf16[16,2048]{1,0:T(8,128)(2,1)S(1)}, bf16[16,2048]{1,0:T(8,128)(2,1)}, u32[]{:S(2)}) copy-start(bf16[16,2048]{1,0:T(8,128)(2,1)} %param.17) | copy-start | bytes 196612
  11.3 7.2 %copy-start.9 = (bf16[2048,2,128]{2,1,0:T(2,128)(2,1)S(1)}, bf16[2048,2,128]{2,1,0:T(2,128)(2,1)}, u32[]{:S(2)}) copy-start(bf16[2048,2,128]{2,1,0:T(2,128)(2,1)} %param.24) | copy-start | bytes 3145732
  11.3 7.2 %copy-start.10 = (f32[2048]{0:T(1024)S(1)}, f32[2048]{0:T(1024)}, u32[]{:S(2)}) copy-start(f32[2048]{0:T(1024)} %param.21) | copy-start | bytes 24580
  17.2 1.6 %copy-start.5 = (f32[2]{0:T(128)S(1)}, f32[2]{0:T(128)}, u32[]{:S(2)}) copy-start(f32[2]{0:T(128)} %param.25) | copy-start | bytes 28
  19.0 5.0 %copy-start.1 = (bf16[2,128,2048]{2,1,0:T(8,128)(2,1)S(1)}, bf16[2,128,2048]{2,1,0:T(8,128)(2,1)}, u32[]{:S(2)}) copy-start(bf16[2,128,2048]{2,1,0:T(8,128)(2,1)} %param.27) | copy-start | bytes 3145732
  19.0 5.0 %copy-start.7 = (f32[128]{0:T(128)S(1)}, f32[128]{0:T(128)}, u32[]{:S(2)}) copy-start(f32[128]{0:T(128)} %param.26) | copy-start | bytes 1540
  19.0 6.0 %copy-start.4 = (s32[16,4]{0,1:T(4,128)S(1)}, s32[16,4]{0,1:T(4,128)}, u32[]{:S(2)}) copy-start(s32[16,4]{0,1:T(4,128)} %param.32) | copy-start | bytes 772
  19.1 41.3 %copy-start.3 = (f32[2048]{0:T(1024)S(1)}, f32[2048]{0:T(1024)}, u32[]{:S(2)}) copy-start(f32[2048]{0:T(1024)} %param.28) | copy-start | bytes 24580
  25.0 79.8 %reduce-scatter.2.cloned.1.call-start = ((), (), s32[]{:S(2)}) async-start(), calls=%async_computation.4 | async-start | bytes 655360 | tf_op jit(solution)/shard_map/reduce_scatter | solution.py:138
  82.2 28.1 %copy-start.6 = (f32[16,4]{0,1:T(4,128)S(1)}, f32[16,4]{0,1:T(4,128)}, u32[]{:S(2)}) copy-start(f32[16,4]{0,1:T(4,128)} %param.33) | copy-start | bytes 772
  104.8 12.8 %all-to-all-start.1 = ((bf16[8,16,512]{2,1,0:T(8,128)(2,1)}), bf16[8,16,512]{2,1,0:T(8,128)(2,1)S(1)}, u32[]{:S(2)}, u32[]{:S(2)}) async-start(bf16[8,16,512]{2,1,0:T(8,128)(2,1)} %reduce-scatter.2.cloned.1.call-done), calls=%async_computation.2 | async-start | bytes 262144 | tf_op jit(solution)/shard_map/all_to_all | solution.py:144
Sparse Core Ops, SparseCore 0:
  25.1 34.2 all-reduce.1
  85.6 19.1 reduce-scatter.1
where the time goes:
time: 126 us; the launch traced here: 125 us
  waiting for transfers between devices  60.2 us (48%)
  matrix products  21.5 us (17%)
  blocking collectives  19.1 us (15%)
  between operations  13.7 us (11%)
  starting transfers between devices  5.55 us (4%)
  other arithmetic  3.87 us (3%)
  local copies, waits for them, and re-layouts  1.29 us (1%)
    psum x1, waiting for transfers between devices, per_device(): lax.psum(partial_value.astype(jnp.bfloat16), 'tp').astype(jnp.float32)  33.8 us
    reduce_scatter x1, waiting for transfers between devices, per_device(): lax.psum_scatter(pieces.reshape(sources, slot_count, model_width).astype(...  19.2 us
    all_to_all x1, blocking collectives, per_device(): lax.all_to_all(own_block, 'ep', split_axis=0, concat_axis=0, tiled=True)  12.7 us
    all_to_all x1, waiting for transfers between devices, per_device(): lax.all_to_all(summed, 'ep', split_axis=0, concat_axis=0, tiled=True)  7.24 us
    all_gather x1, blocking collectives, per_device(): lax.all_gather(lax.all_to_all(own_block, 'ep', split_axis=0, concat_axis=...  6.49 us
    dot_general x1, matrix products, per_device(): jnp.einsum('shcd,slhd->shcl', stacked_query, key_cache, preferred_element...  5.84 us
    all_to_all x1, starting transfers between devices, per_device(): lax.all_to_all(summed, 'ep', split_axis=0, concat_axis=0, tiled=True)  5.5 us
    dot_general x1, matrix products, per_device(): jnp.einsum('shl,slhd->shd', mix_weights, value_cache, preferred_element_t...  4.8 us
  transfers between devices with their start and end apart: 3, of which 3 were waited for; matrix products, arithmetic and copies ran while one was open for 1% of the time, Pallas kernels for 0%

commit v1 on v0

--- a/solution.py
+++ b/solution.py
@@ -99,7 +99,9 @@
         preferred_element_type=jnp.float32,
     )
     partial_value = lax.optimization_barrier(partial_value.astype(jnp.bfloat16)).astype(jnp.float32)
-    attention = lax.psum(partial_value.astype(jnp.bfloat16), "tp").astype(jnp.float32)
+    attention = jnp.sum(lax.all_gather(partial_value.astype(jnp.bfloat16), "tp"), axis=0).astype(
+        jnp.float32
+    )
     residual = (tokens.astype(jnp.float32) + attention).astype(jnp.bfloat16)
     normed_ffn = norm_rows(residual, ffn_gain).astype(jnp.bfloat16)
     experts = lax.axis_size("ep")

time: 126 us -> 98.9 us (0.78)
  waiting for transfers between devices: 60.2 us -> 26.6 us
  blocking collectives: 19.1 us -> 27.5 us
    psum x1 -> x0, waiting for transfers between devices: 33.8 us -> none  [per_device(): lax.psum(partial_value.astype(jnp.bfloat16), 'tp').astype(jnp.float32)]
    all_gather x0 -> x1, blocking collectives: none -> 7.25 us  [per_device(): lax.all_gather(partial_value.astype(jnp.bfloat16), 'tp')]
  transfers between devices with their start and end apart: 3 -> 2, of which waited for: 3 -> 2; matrix products, arithmetic and copies ran while one was open for 1% -> 0% of each run, Pallas kernels for 0% -> 0%
where the time goes in v1:
time: 98.9 us; the launch traced here: 98.6 us
  blocking collectives  27.5 us (28%)
  waiting for transfers between devices  26.6 us (27%)
  matrix products  20.9 us (21%)
  between operations  13.7 us (14%)
  starting transfers between devices  5.51 us (6%)
  other arithmetic  3.08 us (3%)
  local copies, waits for them, and re-layouts  1.28 us (1%)
    reduce_scatter x1, waiting for transfers between devices, per_device(): lax.psum_scatter(pieces.reshape(sources, slot_count, model_width).astype(...  19.3 us
    all_to_all x1, blocking collectives, per_device(): lax.all_to_all(own_block, 'ep', split_axis=0, concat_axis=0, tiled=True)  13.1 us
    all_gather x1, blocking collectives, per_device(): lax.all_gather(partial_value.astype(jnp.bfloat16), 'tp')  7.25 us
    all_to_all x1, waiting for transfers between devices, per_device(): lax.all_to_all(summed, 'ep', split_axis=0, concat_axis=0, tiled=True)  7.24 us
    all_gather x1, blocking collectives, per_device(): lax.all_gather(lax.all_to_all(own_block, 'ep', split_axis=0, concat_axis=...  7.19 us
    dot_general x1, matrix products, per_device(): jnp.einsum('shcd,slhd->shcl', stacked_query, key_cache, preferred_element...  5.84 us
    all_to_all x1, starting transfers between devices, per_device(): lax.all_to_all(summed, 'ep', split_axis=0, concat_axis=0, tiled=True)  5.51 us
    dot_general x1, matrix products, per_device(): jnp.einsum('shl,slhd->shd', mix_weights, value_cache, preferred_element_t...  4.8 us
  transfers between devices with their start and end apart: 2, of which 2 were waited for; matrix products, arithmetic and copies ran while one was open for 0% of the time, Pallas kernels for 0%

profile of v1, /device:TPU:0, one launch (start us, length us, event | category | flops | bytes accessed | tf_op | source)
XLA Modules:
  0.0 98.6 jit_solution(4653368464016129045)
XLA Ops:
  6.6 1.1 %fusion.55 = f32[16]{0:T(128)S(1)} fusion(bf16[16,2048]{1,0:T(8,128)(2,1)} %param.17), kind=kLoop, calls=%fused_computation.50 | loop fusion | flops 98288 | bytes 65600 | tf_op jit(solution)/shard_map/reduce_sum | solution.py:14
  7.7 1.6 %convolution_convert_fusion.4 = bf16[16,256]{1,0:T(8,128)(2,1)S(1)} fusion(bf16[256,8,2,128]{3,2,1,0:T(2,128)(2,1)} %bitcast.112, bf16[16,2048]{1,0:T(8,128)(2,1)} %param.17, f32[2048]{0:T(1024)} %param.21, f32[16]{0:T(128)S(1)} %add_rsqrt_fusion.2), kind=kOutput, calls=%fused_computation.26 | convolution fusion | flops 16912384 | bytes 1130560 | tf_op jit(solution)/shard_map/dot_general | solution.py:57
  9.3 1.6 %convolution_convert_fusion.3 = bf16[16,256]{1,0:T(8,128)(2,1)S(1)} fusion(bf16[256,8,2,128]{3,2,1,0:T(2,128)(2,1)} %bitcast.113, bf16[16,2048]{1,0:T(8,128)(2,1)} %param.17, f32[2048]{0:T(1024)} %param.21, f32[16]{0:T(128)S(1)} %add_rsqrt_fusion.2), kind=kOutput, calls=%fused_computation.25 | convolution fusion | flops 16912384 | bytes 1130560 | tf_op jit(solution)/shard_map/dot_general | solution.py:62
  11.0 0.1 fusion.90
  11.1 0.1 copy.68
  11.2 0.1 iota_compare_fusion.1
  11.3 0.0 copy-start.2
  11.3 0.0 copy-start.9
  11.3 0.0 copy-start.10
  11.3 5.8 %fusion.89 = (f32[16,2,2]{2,1,0:T(2,128)S(1)}, f32[16,2,2,1024]{3,2,1,0:T(2,128)S(1)}) fusion(bf16[16,2,2,128]{3,2,1,0:T(2,128)(2,1)S(1)} %pad_maximum_fusion, bf16[16,1024,2,128]{3,2,1,0:T(2,128)(2,1)} %param.19, pred[16,1024]{1,0:T(8,128)(4,1)S(1)} %iota_compare_fusion.1), kind=kOutput, calls=%fused_computation.105 | convolution fusion | flops 16973760 | bytes 8683776 | tf_op jit(solution)/shard_map/shcd,slhd->shcl/dot_general | solution.py:81
  17.2 0.0 copy-start.5
  17.2 0.1 copy.59
  17.3 0.1 copy.60
  17.4 0.3 fusion.51
  17.7 0.1 copy.61
  17.8 0.1 copy.62
  17.9 0.3 fusion.50
  18.2 0.2 fusion.88
  18.5 0.3 fusion.35
  18.8 0.1 bitcast_convert_fusion
  18.9 0.2 fusion.66
  19.0 0.0 copy-start.3
  19.1 4.8 %fusion = f32[16,2,1,128]{3,2,1,0:T(1,128)S(1)} fusion(bf16[16,1024,2,128]{3,2,1,0:T(2,128)(2,1)} %param.20, bf16[16,2,1024,1]{2,1,0,3:T(2,128)(2,1)S(1)} %fusion.66), kind=kOutput, calls=%fused_computation | convolution fusion | flops 8388608 | bytes 8470528 | tf_op jit(solution)/shard_map/shl,slhd->shd/dot_general | solution.py:86
  23.9 0.2 multiply_reduce_fusion
  24.0 0.3 fusion.4
  24.3 7.2 %all-gather = bf16[64,2048]{1,0:T(8,128)(2,1)S(1)} all-gather(bf16[16,2048]{1,0:T(8,128)(2,1)S(1)} %fusion.4), channel_id=2, replica_groups=mesh['ep'=8,'tp'=4] {'tp'}, dimensions={0}, use_global_device_ids=true | all-gather | bytes 327680 | tf_op jit(solution)/shard_map/all_gather | solution.py:102
  31.6 0.1 fusion.52
  31.8 0.1 fusion.54
  31.9 0.1 broadcast_in_dim.16
  32.0 0.1 reshape.137
  32.1 0.1 copy.65
  32.1 0.1 eq.20
  32.2 0.1 fusion.68
  32.3 0.1 reduce_window_sum.11
  32.4 0.2 select_reduce_fusion.1
  32.6 0.3 convolution_convert_fusion.1
  32.9 13.1 %all_to_all.10 = bf16[8,16,512]{2,1,0:T(8,128)(2,1)S(1)} all-to-all(bf16[8,16,512]{2,1,0:T(8,128)(2,1)S(1)} %constant_dynamic-slice_fusion), channel_id=1, replica_groups=mesh['ep'=8,'tp'=4] {'ep'}, dimensions={0} | all-to-all | bytes 262144 | tf_op jit(solution)/shard_map/all_to_all | solution.py:122
  46.0 7.2 %all_gather.11 = bf16[8,16,2048]{2,1,0:T(8,128)(2,1)S(1)} all-gather(bf16[8,16,512]{2,1,0:T(8,128)(2,1)S(1)} %all_to_all.10), channel_id=1, replica_groups=mesh['ep'=8,'tp'=4] {'tp'}, dimensions={2}, use_global_device_ids=true | all-gather | bytes 655360 | tf_op jit(solution)/shard_map/all_gather | solution.py:121
  53.2 2.1 %fusion.13 = f32[128,512]{1,0:T(8,128)S(1)} fusion(bf16[128,2048]{1,0:T(8,128)(2,1)S(1)} %bitcast.106, bf16[1,2048,512]{2,1,0:T(8,128)(2,1)} %param.29), kind=kOutput, calls=%fused_computation.14 | convolution fusion | flops 268500992 | bytes 2883584 | tf_op jit(solution)/shard_map/dot_general | solution.py:130
  55.3 3.3 %convolution_convert_fusion = bf16[128,2048]{1,0:T(8,128)(2,1)} fusion(bf16[1,512,2048]{2,1,0:T(8,128)(2,1)S(1)} %copy-done, f32[128,512]{1,0:T(8,128)S(1)} %fusion.13, bf16[128,2048]{1,0:T(8,128)(2,1)S(1)} %bitcast.107, bf16[1,2048,512]{2,1,0:T(8,128)(2,1)} %param.30), kind=kOutput, calls=%fused_computation.4 | convolution fusion | flops 537722880 | bytes 5505024 | tf_op jit(solution)/shard_map/dot_general | solution.py:138
  58.6 0.0 reduce-scatter.2.cloned.1.call-update
  58.6 0.1 reduce_sum.73
  58.7 0.1 copy.66
  58.8 19.3 %reduce-scatter.2.cloned.1.call-done = bf16[8,16,512]{2,1,0:T(8,128)(2,1)} async-done(((bf16[8,16,2048]{2,1,0:T(8,128)(2,1)}), bf16[8,16,512]{2,1,0:T(8,128)(2,1)}) %reduce-scatter.2.cloned.1.call-update) | async-done | bytes 131088 | tf_op jit(solution)/shard_map/reduce_scatter | solution.py:140
  78.1 5.5 %all-to-all-start.1 = ((bf16[8,16,512]{2,1,0:T(8,128)(2,1)}), bf16[8,16,512]{2,1,0:T(8,128)(2,1)S(1)}, u32[]{:S(2)}, u32[]{:S(2)}) async-start(bf16[8,16,512]{2,1,0:T(8,128)(2,1)} %reduce-scatter.2.cloned.1.call-done), calls=%async_computation.2 | async-start | bytes 262144 | tf_op jit(solution)/shard_map/all_to_all | solution.py:146
  83.6 0.1 select_reduce_fusion
  83.7 7.2 %all-to-all-done.1 = bf16[8,16,512]{2,1,0:T(8,128)(2,1)S(1)} async-done(((bf16[8,16,512]{2,1,0:T(8,128)(2,1)}), bf16[8,16,512]{2,1,0:T(8,128)(2,1)S(1)}, u32[]{:S(2)}, u32[]{:S(2)}) %all-to-all-start.1) | async-done | bytes 131104 | tf_op jit(solution)/shard_map/all_to_all | solution.py:146
  90.9 0.8 fusion.33
  (33 shorter events, 0.3 us)
Async XLA Ops:
  6.5 48.8 %copy-start = (bf16[1,512,2048]{2,1,0:T(8,128)(2,1)S(1)}, bf16[1,512,2048]{2,1,0:T(8,128)(2,1)}, u32[]{:S(2)}) copy-start(bf16[1,512,2048]{2,1,0:T(8,128)(2,1)} %param.31) | copy-start | bytes 6291460
  6.5 4.7 %copy-start.8 = (s32[16]{0:T(128)S(1)}, s32[16]{0:T(128)}, u32[]{:S(2)}) copy-start(s32[16]{0:T(128)} %param.18) | copy-start | bytes 196
  6.5 71.5 %reduce-scatter.2.cloned.1.call-start = ((), (), s32[]{:S(2)}) async-start(), calls=%async_computation.3 | async-start | bytes 655360 | tf_op jit(solution)/shard_map/reduce_scatter | solution.py:140
  11.3 7.2 %copy-start.2 = (bf16[16,2048]{1,0:T(8,128)(2,1)S(1)}, bf16[16,2048]{1,0:T(8,128)(2,1)}, u32[]{:S(2)}) copy-start(bf16[16,2048]{1,0:T(8,128)(2,1)} %param.17) | copy-start | bytes 196612
  11.3 7.2 %copy-start.9 = (bf16[2048,2,128]{2,1,0:T(2,128)(2,1)S(1)}, bf16[2048,2,128]{2,1,0:T(2,128)(2,1)}, u32[]{:S(2)}) copy-start(bf16[2048,2,128]{2,1,0:T(2,128)(2,1)} %param.24) | copy-start | bytes 3145732
  11.3 7.2 %copy-start.10 = (f32[2048]{0:T(1024)S(1)}, f32[2048]{0:T(1024)}, u32[]{:S(2)}) copy-start(f32[2048]{0:T(1024)} %param.21) | copy-start | bytes 24580
  17.2 1.6 %copy-start.5 = (f32[2]{0:T(128)S(1)}, f32[2]{0:T(128)}, u32[]{:S(2)}) copy-start(f32[2]{0:T(128)} %param.25) | copy-start | bytes 28
  19.0 5.0 %copy-start.1 = (bf16[2,128,2048]{2,1,0:T(8,128)(2,1)S(1)}, bf16[2,128,2048]{2,1,0:T(8,128)(2,1)}, u32[]{:S(2)}) copy-start(bf16[2,128,2048]{2,1,0:T(8,128)(2,1)} %param.27) | copy-start | bytes 3145732
  19.0 5.0 %copy-start.7 = (f32[128]{0:T(128)S(1)}, f32[128]{0:T(128)}, u32[]{:S(2)}) copy-start(f32[128]{0:T(128)} %param.26) | copy-start | bytes 1540
  19.0 12.7 %copy-start.3 = (f32[2048]{0:T(1024)S(1)}, f32[2048]{0:T(1024)}, u32[]{:S(2)}) copy-start(f32[2048]{0:T(1024)} %param.28) | copy-start | bytes 24580
  23.9 8.2 %copy-start.4 = (s32[16,4]{0,1:T(4,128)S(1)}, s32[16,4]{0,1:T(4,128)}, u32[]{:S(2)}) copy-start(s32[16,4]{0,1:T(4,128)} %param.32) | copy-start | bytes 772
  55.3 28.3 %copy-start.6 = (f32[16,4]{0,1:T(4,128)S(1)}, f32[16,4]{0,1:T(4,128)}, u32[]{:S(2)}) copy-start(f32[16,4]{0,1:T(4,128)} %param.33) | copy-start | bytes 772
  78.1 12.9 %all-to-all-start.1 = ((bf16[8,16,512]{2,1,0:T(8,128)(2,1)}), bf16[8,16,512]{2,1,0:T(8,128)(2,1)S(1)}, u32[]{:S(2)}, u32[]{:S(2)}) async-start(bf16[8,16,512]{2,1,0:T(8,128)(2,1)} %reduce-scatter.2.cloned.1.call-done), calls=%async_computation.2 | async-start | bytes 262144 | tf_op jit(solution)/shard_map/all_to_all | solution.py:146
Sparse Core Ops, SparseCore 0:
  58.7 19.3 reduce-scatter.1
